TPU v7x, 32 devices: a whole 2x2x4 slice. The times are simulated.
32 devices in a mesh: ep: 8 (over z, y), tp: 4 (over x, core).
Axes of the slice: x: 2, y: 2, z: 4, core: 2. Of those that a mesh axis runs over, the one named last changes fastest.
Arguments:
- tokens: bfloat16 [2048, 2048], P('ep'), may hold values from -6 to 6
- expert_ids: int32 [2048, 2], P('ep'), may hold values from 0 to 7, all different within a row; in each aligned block of 256 rows (0 to 255, 256 to 511, ...) at most 192 rows name the same one
- route_weight: float32 [2048, 2], P('ep'), may hold values from 0.1 to 1
- norm_gain: float32 [2048], replicated, may hold values from 0.1 to 1.9
- expert_gate: bfloat16 [8, 2048, 2048], P('ep', None, 'tp'), may hold values from -4 to 4
- expert_up: bfloat16 [8, 2048, 2048], P('ep', None, 'tp'), may hold values from -4 to 4
- expert_down: bfloat16 [8, 2048, 2048], P('ep', 'tp'), may hold values from -0.03125 to 0.03125
Outputs:
- combined: bfloat16 [2048, 2048], P('ep', 'tp')
Inputs may be any that keep to these rules, and one draw needn't show every extreme that they name: `expert_ids`: each row names 2 different experts. In each aligned block of 256 rows (the rows of one index of ep) no expert is named by more than 192 rows, and in some block one expert is named by exactly 192 rows.
All inputs are finite; a program needn't handle non-finite values.
Results may differ from a plain program's by a relative error of at most 0.012.
Values may be sent and summed in bfloat16 or wider, within the bound.
A program may use at most 128 MiB of HBM per device.

v0:
```python
import jax
import jax.numpy as jnp
from jax import lax
from jax.sharding import PartitionSpec as P

NORM_EPS = 1e-06
CLAMP_LIMIT = 7.0
SWISH_SCALE = 1.702


def normalize(tokens, norm_gain):
    values = tokens.astype(jnp.float32)
    scaled = values * lax.rsqrt(jnp.mean(values * values, axis=-1, keepdims=True) + NORM_EPS)
    return (scaled * norm_gain).astype(jnp.bfloat16)


def activate(gate_sum, up_sum):
    gate_cut = jnp.minimum(gate_sum, CLAMP_LIMIT)
    up_cut = jnp.clip(up_sum, -CLAMP_LIMIT, CLAMP_LIMIT)
    return ((up_cut + 1.0) * gate_cut * jax.nn.sigmoid(SWISH_SCALE * gate_cut)).astype(jnp.bfloat16)


def shards(tokens, expert_ids, route_weight, norm_gain, expert_gate, expert_up, expert_down):
    groups = lax.axis_size("ep")
    tp_count = lax.axis_size("tp")
    member_count = expert_gate.shape[0]
    experts = groups * member_count
    tok_count, model_width = tokens.shape
    top_count = expert_ids.shape[1]
    capacity = min(tok_count, 3 * tok_count * top_count // experts)
    quarter = model_width // tp_count
    normed = normalize(tokens, norm_gain)
    flat_ids = expert_ids.reshape(-1)
    onehot = (flat_ids[:, None] == jnp.arange(experts, dtype=jnp.int32)[None, :]).astype(jnp.int32)
    slot_index = jnp.sum(jnp.cumsum(onehot, axis=0) * onehot, axis=1) - 1
    position = flat_ids * capacity + slot_index
    token_index = jnp.arange(flat_ids.shape[0], dtype=jnp.int32) // top_count
    row_table = jnp.full((experts * capacity,), tok_count, jnp.int32).at[position].set(token_index)
    padded = jnp.concatenate([normed, jnp.zeros((1, model_width), jnp.bfloat16)], axis=0)
    offset = lax.axis_index("tp") * quarter
    source_rows = lax.dynamic_slice_in_dim(padded, offset, quarter, 1)
    send_rows = source_rows[row_table].reshape(groups, member_count, capacity, quarter)
    received = lax.all_to_all(send_rows, "ep", split_axis=0, concat_axis=0, tiled=True)
    slot_count = received.shape[2]
    shard_piece = lax.all_gather(received, "tp", axis=3, tiled=True)
    span_size = shard_piece.shape[3]
    member = 0
    row_block = shard_piece[:, member].reshape(-1, span_size)
    gate_rows = expert_gate[member]
    up_rows = expert_up[member]
    gate_list = [jnp.dot(row_block, gate_rows, preferred_element_type=jnp.float32)]
    up_list = [jnp.dot(row_block, up_rows, preferred_element_type=jnp.float32)]
    gate_sum = jnp.stack(gate_list)
    up_sum = jnp.stack(up_list)
    activated = activate(gate_sum, up_sum)
    member = 0
    weight_rows = expert_down[member]
    product = lax.dot_general(
        weight_rows, activated[member], (((0,), (1,)), ((), ())), preferred_element_type=jnp.float32
    )
    term_list = [product.reshape(quarter * lax.axis_size("tp"), groups, slot_count)]
    summed = lax.psum_scatter(
        jnp.stack(term_list, axis=2).astype(jnp.bfloat16), "tp", scatter_dimension=0, tiled=True
    )
    returned = lax.all_to_all(
        summed.reshape(quarter, experts * capacity), "ep", split_axis=1, concat_axis=1, tiled=True
    )
    picked = jnp.take(returned, position, axis=1).reshape(quarter, tok_count, top_count)
    weighted = jnp.sum(picked.astype(jnp.float32) * route_weight[None, :, :], axis=2)
    return weighted.T.astype(jnp.bfloat16)


def solution(mesh):
    return jax.shard_map(
        shards,
        mesh=mesh,
        in_specs=(
            P("ep", None),
            P("ep", None),
            P("ep", None),
            P(),
            P("ep", None, "tp"),
            P("ep", None, "tp"),
            P("ep", "tp", None),
        ),
        out_specs=P("ep", "tp"),
        check_vma=False,
    )
```

profile of v0, /device:TPU:0, one launch (start us, length us, event | category | flops | bytes accessed | tf_op | source)
XLA Modules:
  0.0 245.8 jit_solution(14064720156240668413)
XLA Ops:
  6.5 0.0 copy-start
  6.5 0.0 all-gather.2.cloned.1.call-start
  6.5 1.0 copy.19
  7.5 0.1 eq.26
  7.7 0.1 reshape.111
  7.8 0.7 broadcast_multiply_fusion
  8.5 1.1 reduce-window.6
  9.6 0.2 slice_reduce_fusion
  9.9 0.1 fusion.12
  10.0 0.1 copy.23
  10.1 0.1 mul.76
  10.3 2.5 scatter_custom_fusion
  12.8 1.5 fusion.4
  14.3 1.5 fusion.6
  15.9 5.4 %gather_fusion = bf16[1536,512]{1,0:T(8,128)(2,1)} fusion(bf16[257,512]{1,0:T(8,128)(2,1)S(1)} %pad_dynamic-slice_fusion, s32[2048]{0:T(1024)S(1)} %pad_clamp_fusion), kind=kCustom, calls=%fused_computation | custom fusion | bytes 3151872 | tf_op jit(solution)/shard_map/gather | solution.py:42
  21.3 44.4 %all_to_all.17 = bf16[8,1,192,512]{3,2,1,0:T(8,128)(2,1)} all-to-all(bf16[8,1,192,512]{3,2,1,0:T(8,128)(2,1)} %bitcast.37), channel_id=1, replica_groups=mesh['ep'=8,'tp'=4] {'ep'}, dimensions={0} | all-to-all | bytes 3145728 | tf_op jit(solution)/shard_map/all_to_all | solution.py:43
  65.7 0.0 all-gather.2.cloned.1.call-update
  65.8 0.0 reduce-scatter.2.cloned.1.call-start
  65.8 45.5 %all-gather.2.cloned.1.call-done = bf16[8,1,192,2048]{3,2,1,0:T(8,128)(2,1)} async-done(((bf16[8,1,192,512]{3,2,1,0:T(8,128)(2,1)}), bf16[8,1,192,2048]{3,2,1,0:T(8,128)(2,1)}) %all-gather.2.cloned.1.call-update) | async-done | bytes 6291472 | tf_op jit(solution)/shard_map/all_gather | solution.py:45
  111.3 8.5 %convolution_minimum_fusion = f32[1536,512]{1,0:T(8,128)} fusion(bf16[1536,2048]{1,0:T(8,128)(2,1)} %bitcast.43, bf16[1,2048,512]{2,1,0:T(8,128)(2,1)} %param.11), kind=kOutput, calls=%fused_computation.5 | convolution fusion | flops 3222011904 | bytes 11534336 | tf_op jit(solution)/shard_map/dot_general | solution.py:51
  119.8 0.0 copy-done
  119.8 11.9 %convolution_convert_fusion = bf16[1536,2048]{1,0:T(8,128)(2,1)} fusion(bf16[1,512,2048]{2,1,0:T(8,128)(2,1)S(1)} %copy-done, f32[1536,512]{1,0:T(8,128)} %convolution_minimum_fusion, bf16[1536,2048]{1,0:T(8,128)(2,1)} %bitcast.44, bf16[1,2048,512]{2,1,0:T(8,128)(2,1)} %param.12), kind=kOutput, calls=%fused_computation.3 | convolution fusion | flops 6452674560 | bytes 19922944 | tf_op jit(solution)/shard_map/dot_general | solution.py:58
  131.7 0.0 reduce-scatter.2.cloned.1.call-update
  131.7 0.0 copy-start.1
  131.7 0.0 copy-start.2
  131.7 58.0 %reduce-scatter.2.cloned.1.call-done = bf16[512,8,1,192]{0,3,1,2:T(8,128)(2,1)} async-done(((bf16[2048,8,1,192]{0,3,1,2:T(8,128)(2,1)}), bf16[512,8,1,192]{0,3,1,2:T(8,128)(2,1)}) %reduce-scatter.2.cloned.1.call-update) | async-done | bytes 1572880 | tf_op jit(solution)/shard_map/reduce_scatter | solution.py:62
  189.7 5.5 %all-to-all-start.1 = ((bf16[512,8,192]{0,2,1:T(8,128)(2,1)}), bf16[512,8,192]{0,2,1:T(8,128)(2,1)}, u32[]{:S(2)}, u32[]{:S(2)}) async-start(bf16[512,8,192]{0,2,1:T(8,128)(2,1)} %bitcast.39), calls=%async_computation.2 | async-start | bytes 3145728 | tf_op jit(solution)/shard_map/all_to_all | solution.py:65
  195.2 0.1 sub.15
  195.4 0.1 copy.21
  195.5 0.0 copy-done.1
  195.5 0.2 copy.22
  195.7 0.0 copy-done.2
  195.7 0.1 copy.25
  195.8 36.3 %all-to-all-done.1 = bf16[512,8,192]{0,2,1:T(8,128)(2,1)} async-done(((bf16[512,8,192]{0,2,1:T(8,128)(2,1)}), bf16[512,8,192]{0,2,1:T(8,128)(2,1)}, u32[]{:S(2)}, u32[]{:S(2)}) %all-to-all-start.1) | async-done | bytes 1572896 | tf_op jit(solution)/shard_map/all_to_all | solution.py:65
  232.2 3.6 %gather_fusion.1 = bf16[512,512]{1,0:T(8,128)(2,1)S(1)} fusion(bf16[512,1536]{0,1:T(8,128)(2,1)} %bitcast.13, s32[1024]{0:T(1024)S(1)} %pad_clamp_fusion.1), kind=kCustom, calls=%fused_computation.1 | custom fusion | bytes 1050624 | tf_op jit(solution)/shard_map/jit(_take)/gather | solution.py:68
  235.8 0.2 gather.11
  236.0 2.9 %multiply_reduce_fusion = bf16[512,256]{0,1:T(8,128)(2,1)} fusion(bf16[512,256,2]{0,2,1:T(2,128)(2,1)S(1)} %gather.11, pred[256,2]{1,0:T(8,128)(4,1)S(1)} %copy.22, f32[256,2]{1,0:T(8,128)S(1)} %copy.25), kind=kLoop, calls=%fused_computation.19 | loop fusion | flops 917504 | bytes 788992 | tf_op jit(solution)/shard_map/reduce_sum | solution.py:69
  (12 shorter events, 0.1 us)
Async XLA Ops:
  6.5 113.3 %copy-start = (bf16[1,512,2048]{2,1,0:T(8,128)(2,1)S(1)}, bf16[1,512,2048]{2,1,0:T(8,128)(2,1)}, u32[]{:S(2)}) copy-start(bf16[1,512,2048]{2,1,0:T(8,128)(2,1)} %param.13) | copy-start | bytes 6291460
  6.5 104.7 %all-gather.2.cloned.1.call-start = ((), (), s32[]{:S(2)}) async-start(), calls=%async_computation.3 | async-start | bytes 7864320 | tf_op jit(solution)/shard_map/all_gather | solution.py:45
  65.8 124.0 %reduce-scatter.2.cloned.1.call-start = ((), (), s32[]{:S(2)}) async-start(), calls=%async_computation.4 | async-start | bytes 7864320 | tf_op jit(solution)/shard_map/reduce_scatter | solution.py:62
  131.7 63.8 %copy-start.1 = (s32[256,2]{0,1:T(2,128)S(1)}, s32[256,2]{0,1:T(2,128)}, u32[]{:S(2)}) copy-start(s32[256,2]{0,1:T(2,128)} %param.8) | copy-start | bytes 6148
  131.7 64.0 %copy-start.2 = (f32[256,2]{0,1:T(2,128)S(1)}, f32[256,2]{0,1:T(2,128)}, u32[]{:S(2)}) copy-start(f32[256,2]{0,1:T(2,128)} %param.9) | copy-start | bytes 6148
  189.7 42.4 %all-to-all-start.1 = ((bf16[512,8,192]{0,2,1:T(8,128)(2,1)}), bf16[512,8,192]{0,2,1:T(8,128)(2,1)}, u32[]{:S(2)}, u32[]{:S(2)}) async-start(bf16[512,8,192]{0,2,1:T(8,128)(2,1)} %bitcast.39), calls=%async_computation.2 | async-start | bytes 3145728 | tf_op jit(solution)/shard_map/all_to_all | solution.py:65
Sparse Core Ops, SparseCore 0:
  65.9 45.3 all-gather.1
  131.8 57.8 reduce-scatter.1
where the time goes:
time: 246 us
  waiting for transfers between devices  140 us (57%)
  blocking collectives  44.4 us (18%)
  matrix products  20.4 us (8%)
  local copies, waits for them, and re-layouts  14 us (6%)
  between operations  13.6 us (6%)
  other arithmetic  8.01 us (3%)
  starting transfers between devices  5.56 us (2%)
    reduce_scatter x1, waiting for transfers between devices, shards(): lax.psum_scatter(jnp.stack(term_list, axis=2).astype(jnp.bfloat16), 'tp',...  58 us
    all_gather x1, waiting for transfers between devices, shards(): shard_piece = lax.all_gather(received, 'tp', axis=3, tiled=True)  45.5 us
    all_to_all x1, blocking collectives, shards(): lax.all_to_all(send_rows, 'ep', split_axis=0, concat_axis=0, tiled=True)  44.4 us
    all_to_all x1, waiting for transfers between devices, shards(): lax.all_to_all(summed.reshape(quarter, experts * capacity), 'ep', split_a...  36.3 us
    dot_general x1, matrix products, shards(): lax.dot_general(weight_rows, activated[member], (((0,), (1,)), ((), ())),...  11.9 us
    dot_general x1, matrix products, shards(): jnp.dot(row_block, gate_rows, preferred_element_type=jnp.float32)  8.52 us
    all_to_all x1, starting transfers between devices, shards(): lax.all_to_all(summed.reshape(quarter, experts * capacity), 'ep', split_a...  5.51 us
    gather x1, local copies, waits for them, and re-layouts, shards(): source_rows[row_table].reshape(groups, member_count, capacity, quarter)  5.43 us
  transfers between devices with their start and end apart: 3, of which 3 were waited for; matrix products, arithmetic and copies ran while one was open for 0% of the time, Pallas kernels for 0%

commit v1 on v0

--- a/solution.py
+++ b/solution.py
@@ -62,8 +62,16 @@
     summed = lax.psum_scatter(
         jnp.stack(term_list, axis=2).astype(jnp.bfloat16), "tp", scatter_dimension=0, tiled=True
     )
-    returned = lax.all_to_all(
-        summed.reshape(quarter, experts * capacity), "ep", split_axis=1, concat_axis=1, tiled=True
+    returned = jnp.concatenate(
+        lax.all_to_all(
+            jnp.stack(
+                jnp.split(summed.reshape(quarter, experts * capacity), lax.axis_size("ep"), axis=1)
+            ),
+            "ep",
+            0,
+            0,
+        ),
+        axis=1,
     )
     picked = jnp.take(returned, position, axis=1).reshape(quarter, tok_count, top_count)
     weighted = jnp.sum(picked.astype(jnp.float32) * route_weight[None, :, :], axis=2)

time: 246 us -> 259 us (1.053)
  local copies, waits for them, and re-layouts: 14 us -> 26.9 us
    unnamed x8 -> x17, local copies, waits for them, and re-layouts: 1.11 us -> 12.4 us
where the time goes in v1:
time: 259 us; the launch traced here: 258 us
  waiting for transfers between devices  140 us (54%)
  blocking collectives  44.4 us (17%)
  local copies, waits for them, and re-layouts  26.9 us (10%)
  matrix products  20.4 us (8%)
  between operations  13.6 us (5%)
  other arithmetic  7.47 us (3%)
  starting transfers between devices  5.56 us (2%)
    reduce_scatter x1, waiting for transfers between devices, shards(): lax.psum_scatter(jnp.stack(term_list, axis=2).astype(jnp.bfloat16), 'tp',...  58 us
    all_gather x1, waiting for transfers between devices, shards(): shard_piece = lax.all_gather(received, 'tp', axis=3, tiled=True)  45.5 us
    all_to_all x1, blocking collectives, shards(): lax.all_to_all(send_rows, 'ep', split_axis=0, concat_axis=0, tiled=True)  44.4 us
    all_to_all x1, waiting for transfers between devices, shards(): lax.all_to_all(jnp.stack(jnp.split(summed.reshape(quarter, experts * capa...  36.4 us
    unnamed x17, local copies, waits for them, and re-layouts  12.4 us
    dot_general x1, matrix products, shards(): lax.dot_general(weight_rows, activated[member], (((0,), (1,)), ((), ())),...  11.9 us
    dot_general x1, matrix products, shards(): jnp.dot(row_block, gate_rows, preferred_element_type=jnp.float32)  8.52 us
    all_to_all x1, starting transfers between devices, shards(): lax.all_to_all(jnp.stack(jnp.split(summed.reshape(quarter, experts * capa...  5.52 us
  transfers between devices with their start and end apart: 3, of which 3 were waited for; matrix products, arithmetic and copies ran while one was open for 0% of the time, Pallas kernels for 0%

profile of v1, /device:TPU:0, one launch (start us, length us, event | category | flops | bytes accessed | tf_op | source)
XLA Modules:
  0.0 258.2 jit_solution(4329248123373415777)
XLA Ops:
  6.5 0.0 copy-start
  6.5 0.0 copy-start.1
  6.5 0.0 all-gather.2.cloned.1.call-start
  6.5 1.0 copy.19
  7.5 0.1 eq.26
  7.7 0.1 reshape.116
  7.8 0.7 broadcast_multiply_fusion
  8.5 1.1 reduce-window.6
  9.6 0.2 slice_reduce_fusion
  9.9 0.1 fusion.20
  10.0 0.1 copy.23
  10.1 0.1 mul.76
  10.3 2.5 scatter_custom_fusion
  12.8 1.5 fusion.4
  14.3 0.0 copy-done.1
  14.3 1.0 fusion.6
  15.4 5.4 %gather_fusion = bf16[1536,512]{1,0:T(8,128)(2,1)} fusion(bf16[257,512]{1,0:T(8,128)(2,1)S(1)} %pad_dynamic-slice_fusion, s32[2048]{0:T(1024)S(1)} %pad_clamp_fusion), kind=kCustom, calls=%fused_computation | custom fusion | bytes 3151872 | tf_op jit(solution)/shard_map/gather | solution.py:42
  20.8 44.4 %all_to_all.10 = bf16[8,1,192,512]{3,2,1,0:T(8,128)(2,1)} all-to-all(bf16[8,1,192,512]{3,2,1,0:T(8,128)(2,1)} %bitcast.71), channel_id=1, replica_groups=mesh['ep'=8,'tp'=4] {'ep'}, dimensions={0} | all-to-all | bytes 3145728 | tf_op jit(solution)/shard_map/all_to_all | solution.py:43
  65.2 0.0 all-gather.2.cloned.1.call-update
  65.2 0.0 reduce-scatter.2.cloned.1.call-start
  65.3 45.5 %all-gather.2.cloned.1.call-done = bf16[8,1,192,2048]{3,2,1,0:T(8,128)(2,1)} async-done(((bf16[8,1,192,512]{3,2,1,0:T(8,128)(2,1)}), bf16[8,1,192,2048]{3,2,1,0:T(8,128)(2,1)}) %all-gather.2.cloned.1.call-update) | async-done | bytes 6291472 | tf_op jit(solution)/shard_map/all_gather | solution.py:45
  110.8 8.5 %convolution_minimum_fusion = f32[1536,512]{1,0:T(8,128)} fusion(bf16[1536,2048]{1,0:T(8,128)(2,1)} %bitcast.84, bf16[1,2048,512]{2,1,0:T(8,128)(2,1)} %param.11), kind=kOutput, calls=%fused_computation.5 | convolution fusion | flops 3222011904 | bytes 11534336 | tf_op jit(solution)/shard_map/dot_general | solution.py:51
  119.3 0.0 copy-done
  119.3 11.9 %convolution_convert_fusion = bf16[1536,2048]{1,0:T(8,128)(2,1)} fusion(bf16[1,512,2048]{2,1,0:T(8,128)(2,1)S(1)} %copy-done, f32[1536,512]{1,0:T(8,128)} %convolution_minimum_fusion, bf16[1536,2048]{1,0:T(8,128)(2,1)} %bitcast.85, bf16[1,2048,512]{2,1,0:T(8,128)(2,1)} %param.12), kind=kOutput, calls=%fused_computation.3 | convolution fusion | flops 6452674560 | bytes 19922944 | tf_op jit(solution)/shard_map/dot_general | solution.py:58
  131.2 0.0 reduce-scatter.2.cloned.1.call-update
  131.2 58.0 %reduce-scatter.2.cloned.1.call-done = bf16[512,8,1,192]{0,3,1,2:T(8,128)(2,1)} async-done(((bf16[2048,8,1,192]{0,3,1,2:T(8,128)(2,1)}), bf16[512,8,1,192]{0,3,1,2:T(8,128)(2,1)}) %reduce-scatter.2.cloned.1.call-update) | async-done | bytes 1572880 | tf_op jit(solution)/shard_map/reduce_scatter | solution.py:62
  189.2 1.6 fusion.19
  190.8 1.6 fusion.18
  192.4 1.6 fusion.17
  194.0 1.6 fusion.16
  195.6 1.6 fusion.15
  197.2 1.6 fusion.14
  198.9 0.0 copy-start.2
  198.9 0.0 copy-start.3
  198.9 1.6 fusion.13
  200.5 1.6 fusion.12
  202.1 5.5 %all-to-all-start.1 = ((bf16[8,512,192]{1,2,0:T(8,128)(2,1)}), bf16[8,512,192]{1,2,0:T(8,128)(2,1)}, u32[]{:S(2)}, u32[]{:S(2)}) async-start(bf16[8,512,192]{1,2,0:T(8,128)(2,1)} %fusion.12), calls=%async_computation.2 | async-start | bytes 3145728 | tf_op jit(solution)/shard_map/all_to_all | solution.py:66
  207.6 0.1 sub.15
  207.8 0.1 copy.21
  207.9 0.0 copy-done.2
  207.9 0.2 copy.22
  208.1 0.0 copy-done.3
  208.1 0.1 copy.25
  208.2 36.4 %all-to-all-done.1 = bf16[8,512,192]{1,2,0:T(8,128)(2,1)} async-done(((bf16[8,512,192]{1,2,0:T(8,128)(2,1)}), bf16[8,512,192]{1,2,0:T(8,128)(2,1)}, u32[]{:S(2)}, u32[]{:S(2)}) %all-to-all-start.1) | async-done | bytes 1572896 | tf_op jit(solution)/shard_map/all_to_all | solution.py:66
  244.6 3.6 %gather_fusion.1 = bf16[512,512]{1,0:T(8,128)(2,1)S(1)} fusion(bf16[512,1536]{0,1:T(8,128)(2,1)} %bitcast.22, s32[1024]{0:T(1024)S(1)} %pad_clamp_fusion.1), kind=kCustom, calls=%fused_computation.1 | custom fusion | bytes 1050624 | tf_op jit(solution)/shard_map/jit(_take)/gather | solution.py:76
  248.2 0.2 gather.11
  248.4 2.9 %multiply_reduce_fusion = bf16[512,256]{0,1:T(8,128)(2,1)} fusion(bf16[512,256,2]{0,2,1:T(2,128)(2,1)S(1)} %gather.11, pred[256,2]{1,0:T(8,128)(4,1)S(1)} %copy.22, f32[256,2]{1,0:T(8,128)S(1)} %copy.25), kind=kLoop, calls=%fused_computation.19 | loop fusion | flops 917504 | bytes 788992 | tf_op jit(solution)/shard_map/reduce_sum | solution.py:77
  (12 shorter events, 0.1 us)
Async XLA Ops:
  6.5 112.7 %copy-start = (bf16[1,512,2048]{2,1,0:T(8,128)(2,1)S(1)}, bf16[1,512,2048]{2,1,0:T(8,128)(2,1)}, u32[]{:S(2)}) copy-start(bf16[1,512,2048]{2,1,0:T(8,128)(2,1)} %param.13) | copy-start | bytes 6291460
  6.5 7.8 %copy-start.1 = (bf16[256,2048]{1,0:T(8,128)(2,1)S(1)}, bf16[256,2048]{1,0:T(8,128)(2,1)}, u32[]{:S(2)}) copy-start(bf16[256,2048]{1,0:T(8,128)(2,1)} %param.7) | copy-start | bytes 3145732
  6.5 104.2 %all-gather.2.cloned.1.call-start = ((), (), s32[]{:S(2)}) async-start(), calls=%async_computation.3 | async-start | bytes 7864320 | tf_op jit(solution)/shard_map/all_gather | solution.py:45
  65.2 124.0 %reduce-scatter.2.cloned.1.call-start = ((), (), s32[]{:S(2)}) async-start(), calls=%async_computation.4 | async-start | bytes 7864320 | tf_op jit(solution)/shard_map/reduce_scatter | solution.py:62
  198.9 9.0 %copy-start.2 = (s32[256,2]{0,1:T(2,128)S(1)}, s32[256,2]{0,1:T(2,128)}, u32[]{:S(2)}) copy-start(s32[256,2]{0,1:T(2,128)} %param.8) | copy-start | bytes 6148
  198.9 9.2 %copy-start.3 = (f32[256,2]{0,1:T(2,128)S(1)}, f32[256,2]{0,1:T(2,128)}, u32[]{:S(2)}) copy-start(f32[256,2]{0,1:T(2,128)} %param.9) | copy-start | bytes 6148
  202.1 42.5 %all-to-all-start.1 = ((bf16[8,512,192]{1,2,0:T(8,128)(2,1)}), bf16[8,512,192]{1,2,0:T(8,128)(2,1)}, u32[]{:S(2)}, u32[]{:S(2)}) async-start(bf16[8,512,192]{1,2,0:T(8,128)(2,1)} %fusion.12), calls=%async_computation.2 | async-start | bytes 3145728 | tf_op jit(solution)/shard_map/all_to_all | solution.py:66
Sparse Core Ops, SparseCore 0:
  65.4 45.3 all-gather.1
  131.3 57.8 reduce-scatter.1
